TPU v7x, 512 devices: a whole 4x4x16 slice. The times are simulated.
512 devices in a mesh: sp: 64 (over z, y), tp: 8 (over x, core).
Axes of the slice: x: 4, y: 4, z: 16, core: 2. Of those that a mesh axis runs over, the one named last changes fastest.
Arguments:
- queries: bfloat16 [8192, 1024], P('sp', 'tp'), may hold values from -6 to 6
- attn_out: bfloat16 [8192, 1024], P('sp', 'tp'), may hold values from -6 to 6
- out_grad: bfloat16 [8192, 1024], P('sp', 'tp'), may hold values from -384 to 384
- row_lse: float32 [8192, 8], P('sp', 'tp'), may hold values from 9.5 to 12.5
- source: bfloat16 [32768, 4096], P('sp', 'tp'), may hold values from -6 to 6
- saved_keys: bfloat16 [32768, 256], P('sp'), may hold values from -6 to 6
- saved_values: bfloat16 [32768, 256], P('sp'), may hold values from -6 to 6
- key_weight: bfloat16 [4096, 256], P('tp'), may hold values from -0.09375 to 0.09375
- value_weight: bfloat16 [4096, 256], P('tp'), may hold values from -0.09375 to 0.09375
Outputs:
- query_grad: float32 [8192, 1024], P('sp', 'tp')
- source_grad: float32 [32768, 4096], P('sp', 'tp')
- key_grad: float32 [256, 4096], P('sp', 'tp')
All inputs are finite; a program needn't handle non-finite values.
Results may differ from a plain program's by a relative error of at most 0.012.
Values may be sent and summed in bfloat16 or wider, within the bound.
No kernel may reach another device: no remote copies, remote signals or barrier semaphores. Data moves between devices by JAX's collectives and lax.ppermute only.
A program may use at most 64 MiB of HBM per device.

v0:
```python
import math
import jax
import jax.numpy as jnp
from jax import lax
from jax.sharding import Mesh
from jax.sharding import PartitionSpec as P

HEADS = 8
KV_HEADS = 2
HEAD_DIM = 128
SP = ("sp_0", "sp_1")


def copy_for_each(value, axis):
    size = lax.axis_size(axis)
    return lax.all_to_all(
        jnp.broadcast_to(value[None], (size, *value.shape)), axis, 0, 0, tiled=True
    )


def joined_along(pieces, dim):
    pieces = jnp.moveaxis(pieces, 0, dim)
    lengths = pieces.shape
    return pieces.reshape(*lengths[:dim], lengths[dim] * lengths[dim + 1], *lengths[dim + 2 :])


def gather_directly(value, axis, dim):
    pieces = copy_for_each(value, axis)
    return joined_along(pieces, dim)


def gather_axes(value, axes, dim):
    for axis in reversed(axes):
        value = lax.all_gather(value, axis, axis=dim, tiled=True)
    return value


def together(arrays, axis):
    ends = [0]
    for a in arrays:
        ends.append(ends[-1] + a.size)
    subtotal = lax.psum(jnp.concatenate([a.ravel() for a in arrays]), axis)
    return tuple((subtotal[b:e].reshape(a.shape) for a, b, e in zip(arrays, ends, ends[1:])))


def split_up(value, dim, size):
    before, after = (value.shape[:dim], value.shape[dim + 1 :])
    return jnp.moveaxis(value.reshape(*before, size, -1, *after), dim, 0)


def sum_at_owner(value, axis, dim):
    pieces = split_up(value, dim, lax.axis_size(axis))
    arrived = lax.all_to_all(pieces, axis, split_axis=0, concat_axis=0, tiled=True)
    return arrived.astype(jnp.float32).sum(axis=0)


def contract_rows(left, right):
    return lax.dot_general(
        left, right, (((0,), (0,)), ((), ())), preferred_element_type=jnp.float32
    )


def contract_cols(left, right):
    return lax.dot_general(
        left, right, (((1,), (1,)), ((), ())), preferred_element_type=jnp.float32
    )


def shards(
    queries, attn_out, out_grad, row_lse, source, saved_keys, saved_values, key_weight, value_weight
):
    local_heads = row_lse.shape[1]
    tgt_rows = queries.shape[0]
    width = queries.shape[1]
    src_rows = source.shape[0]
    sp_count = lax.axis_size(SP)
    first_head = lax.axis_index("tp") * local_heads
    per_key = HEADS // KV_HEADS
    score_scale = 1.0 / math.sqrt(HEAD_DIM)
    row_delta = jnp.sum(
        (out_grad.astype(jnp.float32) * attn_out.astype(jnp.float32)).reshape(
            tgt_rows, local_heads, HEAD_DIM
        ),
        axis=2,
    )
    row_blocks = jnp.stack([queries, out_grad])
    row_stats = jnp.stack([row_lse, row_delta])
    whole_stats = gather_directly(row_stats, SP, 1)
    kv_starts = [(first_head + 0) // per_key * HEAD_DIM]
    key_heads = [lax.dynamic_slice_in_dim(saved_keys, start, HEAD_DIM, 1) for start in kv_starts]
    value_heads = [
        lax.dynamic_slice_in_dim(saved_values, start, HEAD_DIM, 1) for start in kv_starts
    ]
    total_rows = tgt_rows * sp_count
    initial = (
        jnp.zeros((total_rows, width), jnp.float32),
        jnp.zeros((src_rows, KV_HEADS * HEAD_DIM), jnp.float32),
        jnp.zeros((src_rows, KV_HEADS * HEAD_DIM), jnp.float32),
    )
    blocks = gather_axes(row_blocks, SP, 1)
    rows = blocks.shape[1]
    span = math.gcd(rows, 1024)
    count = rows // span

    def step(turn, inner):
        query_buf, key_acc, value_acc = inner
        begin = turn * span
        block_rows = lax.dynamic_slice_in_dim(blocks, begin, span, 1)
        block_stats = lax.dynamic_slice_in_dim(whole_stats, begin, span, 1)
        query_head = block_rows[0, :, 0:HEAD_DIM]
        grad_head = block_rows[1, :, 0:HEAD_DIM]
        lse_col = block_stats[0, :, 0:1]
        delta_col = block_stats[1, :, 0:1]
        scores = contract_cols(query_head, key_heads[0]) * score_scale
        attn_probs = jnp.exp(scores - lse_col)
        dprobs = contract_cols(grad_head, value_heads[0])
        dscores = (attn_probs * (dprobs - delta_col) * score_scale).astype(jnp.bfloat16)
        parts = [jnp.dot(dscores, key_heads[0], preferred_element_type=jnp.float32)]
        key_part = contract_rows(dscores, query_head)
        value_part = contract_rows(attn_probs.astype(jnp.bfloat16), grad_head)
        kv_start = kv_starts[0]
        key_acc = lax.dynamic_update_slice_in_dim(
            key_acc,
            lax.dynamic_slice_in_dim(key_acc, kv_start, HEAD_DIM, 1) + key_part,
            kv_start,
            1,
        )
        value_acc = lax.dynamic_update_slice_in_dim(
            value_acc,
            lax.dynamic_slice_in_dim(value_acc, kv_start, HEAD_DIM, 1) + value_part,
            kv_start,
            1,
        )
        query_buf = lax.dynamic_update_slice_in_dim(
            query_buf, jnp.concatenate(parts, axis=1), begin, 0
        )
        return (query_buf, key_acc, value_acc)

    partials, key_acc, value_acc = lax.fori_loop(0, count, step, initial)
    stacked = partials.reshape(sp_count, tgt_rows, width)
    received = lax.all_to_all(
        stacked.astype(jnp.bfloat16), SP, split_axis=0, concat_axis=0, tiled=True
    ).astype(stacked.dtype)
    query_grad = jnp.sum(received, axis=0)
    key_acc, value_acc = tuple(
        (
            part.astype(jnp.float32)
            for part in together(
                (key_acc.astype(jnp.bfloat16), value_acc.astype(jnp.bfloat16)), "tp"
            )
        )
    )
    key_half = key_acc.astype(jnp.bfloat16)
    value_half = value_acc.astype(jnp.bfloat16)
    source_grad = contract_cols(key_half, key_weight) + contract_cols(value_half, value_weight)
    weight_scale = 1.0 / math.sqrt(src_rows * sp_count)
    key_grad = sum_at_owner(
        (contract_rows(key_half, source) * weight_scale).astype(jnp.bfloat16), SP, 0
    )
    return (query_grad, source_grad, key_grad)


def solution(mesh):
    split = Mesh(mesh.devices.reshape(16, 4, mesh.shape["tp"]), ("sp_0", "sp_1", "tp"))
    return jax.shard_map(
        shards,
        mesh=split,
        in_specs=(
            P(SP, "tp"),
            P(SP, "tp"),
            P(SP, "tp"),
            P(SP, "tp"),
            P(SP, "tp"),
            P(SP, None),
            P(SP, None),
            P("tp", None),
            P("tp", None),
        ),
        out_specs=(P(SP, "tp"), P(SP, "tp"), P(SP, "tp")),
        check_vma=False,
    )
```

profile of v0, /device:TPU:6, one launch (start us, length us, event | category | flops | bytes accessed | tf_op | source)
XLA Modules:
  0.0 390.1 jit_solution(9942946184266667918)
XLA Ops:
  7.2 0.8 pad_maximum_fusion.1
  8.1 13.5 %all_gather.6 = bf16[2,512,128]{2,1,0:T(8,128)(2,1)} all-gather(bf16[2,128,128]{2,1,0:T(8,128)(2,1)S(1)} %pad_maximum_fusion.1), channel_id=1, replica_groups=mesh['sp_0'=16,'sp_1'=4,'tp'=8] {'sp_1'}, dimensions={1}, use_global_device_ids=true | all-gather | bytes 327680 | tf_op jit(solution)/shard_map/all_gather | solution.py:34
  21.6 0.9 multiply_reduce_fusion
  22.5 0.7 pad_maximum_fusion.2
  23.1 0.6 broadcast_in_dim.13
  23.8 18.2 %all-to-all-start = ((f32[64,2,128,1]{2,1,3,0:T(2,128)}), f32[64,2,128,1]{2,1,3,0:T(2,128)S(1)}, u32[]{:S(2)}, u32[]{:S(2)}) async-start(f32[64,2,128,1]{2,1,3,0:T(2,128)} %broadcast_in_dim.13), calls=%async_computation | async-start | bytes 131072 | tf_op jit(solution)/shard_map/all_to_all | solution.py:16
  42.1 1.0 constant_dynamic-slice_fusion.2
  43.0 14.7 %all-to-all-done = f32[64,2,128,1]{2,1,3,0:T(2,128)S(1)} async-done(((f32[64,2,128,1]{2,1,3,0:T(2,128)}), f32[64,2,128,1]{2,1,3,0:T(2,128)S(1)}, u32[]{:S(2)}, u32[]{:S(2)}) %all-to-all-start) | async-done | bytes 65568 | tf_op jit(solution)/shard_map/all_to_all | solution.py:16
  57.8 47.4 %all-gather.2.cloned.1.call-done = bf16[2,8192,128]{2,1,0:T(8,128)(2,1)} async-done(((bf16[2,512,128]{2,1,0:T(8,128)(2,1)}), bf16[2,8192,128]{2,1,0:T(8,128)(2,1)}) %all-gather.2.cloned.1.call-update) | async-done | bytes 4194320 | tf_op jit(solution)/shard_map/all_gather | solution.py:34
  105.3 1.5 broadcast_in_dim.11
  106.7 58.4 %while.19 = (s32[]{:T(128)}, bf16[8192,128]{1,0:T(8,128)(2,1)}, f32[512,256]{1,0:T(8,128)S(1)}, f32[512,256]{1,0:T(8,128)S(1)}, bf16[2,8192,128]{2,1,0:T(8,128)(...) while((s32[]{:T(128)}, bf16[8192,128]{1,0:T(8,128)(2,1)}, ...), condition=%wide.region_2.3_spmd, body=%wide.region_1.2_spmd.sunk | while | flops 675938304 | bytes 12481763 | solution.py:139
  106.7 1.4 fusion.41
  108.1 1.7 fusion.43
  109.8 1.6 multiply_convert_fusion.2
  111.4 1.4 fusion.42
  112.9 1.1 convolution_dynamic-update-slice_fusion.2
  114.0 1.4 fusion.41
  115.4 1.7 fusion.43
  117.1 1.6 multiply_convert_fusion.2
  118.7 1.4 fusion.42
  120.2 1.2 convolution_dynamic-update-slice_fusion.2
  121.3 1.4 fusion.41
  122.7 1.7 fusion.43
  124.4 1.6 multiply_convert_fusion.2
  126.1 1.4 fusion.42
  127.5 1.2 convolution_dynamic-update-slice_fusion.2
  128.7 1.4 fusion.41
  130.0 1.7 fusion.43
  131.7 1.6 multiply_convert_fusion.2
  133.4 1.4 fusion.42
  134.8 1.2 convolution_dynamic-update-slice_fusion.2
  136.0 1.4 fusion.41
  137.4 1.7 fusion.43
  139.1 1.6 multiply_convert_fusion.2
  140.7 1.4 fusion.42
  142.1 1.1 convolution_dynamic-update-slice_fusion.2
  143.3 1.4 fusion.41
  144.6 1.7 fusion.43
  146.3 1.6 multiply_convert_fusion.2
  148.0 1.4 fusion.42
  149.4 1.1 convolution_dynamic-update-slice_fusion.2
  150.6 1.4 fusion.41
  151.9 1.7 fusion.43
  153.6 1.6 multiply_convert_fusion.2
  155.3 1.4 fusion.42
  156.7 1.1 convolution_dynamic-update-slice_fusion.2
  157.8 1.4 fusion.41
  159.2 1.7 fusion.43
  160.9 1.6 multiply_convert_fusion.2
  162.6 1.4 fusion.42
  164.0 1.1 convolution_dynamic-update-slice_fusion.2
  165.4 0.2 copy.13
  165.7 0.8 pad_maximum_fusion
  166.5 70.1 %all-reduce.2.cloned.1.call-done = bf16[262144]{0:T(1024)(128)(2,1)} async-done(((bf16[262144]{0:T(1024)(128)(2,1)}), bf16[262144]{0:T(1024)(128)(2,1)}) %all-reduce.2.cloned.1.call-update) | async-done | bytes 524304 | tf_op jit(solution)/shard_map/psum | solution.py:42
  236.6 1.1 fusion.13
  237.8 0.3 fusion.12
  238.1 0.4 copy-done.1
  238.6 38.4 %all_to_all.15 = bf16[64,4,512]{2,1,0:T(4,128)(2,1)S(1)} all-to-all(bf16[64,4,512]{2,1,0:T(4,128)(2,1)S(1)} %reshape.49), channel_id=1, replica_groups=mesh['sp_0'=16,'sp_1'=4,'tp'=8] {'sp_0','sp_1'}, dimensions={0} | all-to-all | bytes 524288 | tf_op jit(solution)/shard_map/all_to_all | solution.py:53
  277.0 5.4 %all-to-all-start.1 = ((bf16[64,128,128]{2,1,0:T(8,128)(2,1)}), bf16[64,128,128]{2,1,0:T(8,128)(2,1)S(1)}, u32[]{:S(2)}, u32[]{:S(2)}) async-start(bf16[64,128,128]{2,1,0:T(8,128)(2,1)} %bitcast.58), calls=%async_computation.1 | async-start | bytes 4194304 | tf_op jit(solution)/shard_map/all_to_all | solution.py:141
  282.5 1.4 fusion.14
  283.9 2.3 convolution_add_fusion.2
  286.1 0.7 convert_reduce_fusion.1
  286.8 95.4 %all-to-all-done.1 = bf16[64,128,128]{2,1,0:T(8,128)(2,1)S(1)} async-done(((bf16[64,128,128]{2,1,0:T(8,128)(2,1)}), bf16[64,128,128]{2,1,0:T(8,128)(2,1)S(1)}, u32[]{:S(2)}, u32[]{:S(2)}) %all-to-all-start.1) | async-done | bytes 2097184 | tf_op jit(solution)/shard_map/all_to_all | solution.py:141
  382.3 0.9 convert_reduce_fusion
  (24 shorter events, 0.8 us)
Async XLA Ops:
  7.2 230.6 %copy-start = (bf16[512,512]{1,0:T(8,128)(2,1)S(1)}, bf16[512,512]{1,0:T(8,128)(2,1)}, u32[]{:S(2)}) copy-start(bf16[512,512]{1,0:T(8,128)(2,1)} %param.15) | copy-start | bytes 1572868
  7.2 98.0 %all-gather.2.cloned.1.call-start = ((), (), s32[]{:S(2)}) async-start(), calls=%async_computation.3 | async-start | bytes 4456448 | tf_op jit(solution)/shard_map/all_gather | solution.py:34
  23.8 34.0 %all-to-all-start = ((f32[64,2,128,1]{2,1,3,0:T(2,128)}), f32[64,2,128,1]{2,1,3,0:T(2,128)S(1)}, u32[]{:S(2)}, u32[]{:S(2)}) async-start(f32[64,2,128,1]{2,1,3,0:T(2,128)} %broadcast_in_dim.13), calls=%async_computation | async-start | bytes 131072 | tf_op jit(solution)/shard_map/all_to_all | solution.py:16
  42.0 194.6 %all-reduce.2.cloned.1.call-start = ((), (), s32[]{:S(2)}) async-start(), calls=%async_computation.4 | async-start | bytes 1048576 | tf_op jit(solution)/shard_map/psum | solution.py:42
  237.8 0.7 copy-start.1
  277.0 105.3 %all-to-all-start.1 = ((bf16[64,128,128]{2,1,0:T(8,128)(2,1)}), bf16[64,128,128]{2,1,0:T(8,128)(2,1)S(1)}, u32[]{:S(2)}, u32[]{:S(2)}) async-start(bf16[64,128,128]{2,1,0:T(8,128)(2,1)} %bitcast.58), calls=%async_computation.1 | async-start | bytes 4194304 | tf_op jit(solution)/shard_map/all_to_all | solution.py:141
Sparse Core Ops, SparseCore 0:
  21.7 83.4 all-gather.1
  166.6 69.9 all-reduce.1
where the time goes:
time: 392 us; the launch traced here: 390 us
  waiting for transfers between devices  228 us (58%)
  matrix products  62.1 us (16%)
  blocking collectives  51.9 us (13%)
  starting transfers between devices  23.6 us (6%)
  between operations  14.2 us (4%)
  local copies, waits for them, and re-layouts  5.3 us (1%)
  other arithmetic  4.95 us (1%)
    all_to_all x1, waiting for transfers between devices, shards(): lax.all_to_all(stacked.astype(jnp.bfloat16), SP, split_axis=0, concat_axi...  95.4 us
    psum x1, waiting for transfers between devices, together(): subtotal = lax.psum(jnp.concatenate([a.ravel() for a in arrays]), axis)  70.1 us
    all_gather x1, waiting for transfers between devices, gather_axes(): value = lax.all_gather(value, axis, axis=dim, tiled=True)  47.4 us
    all_to_all x1, blocking collectives, sum_at_owner(): lax.all_to_all(pieces, axis, split_axis=0, concat_axis=0, tiled=True)  38.4 us
    dot_general x18, matrix products, contract_cols(): lax.dot_general(left, right, (((1,), (1,)), ((), ())), preferred_element_...  27.6 us
    dot_general x17, matrix products, contract_rows(): lax.dot_general(left, right, (((0,), (0,)), ((), ())), preferred_element_...  25.4 us
    all_to_all x1, starting transfers between devices, copy_for_each(): lax.all_to_all(jnp.broadcast_to(value[None], (size, *value.shape)), axis,...  18.2 us
    all_to_all x1, waiting for transfers between devices, copy_for_each(): lax.all_to_all(jnp.broadcast_to(value[None], (size, *value.shape)), axis,...  14.7 us
  transfers between devices with their start and end apart: 4, of which 4 were waited for; matrix products, arithmetic and copies ran while one was open for 2% of the time, Pallas kernels for 0%

commit v1 on v0

--- a/solution.py
+++ b/solution.py
@@ -39,7 +39,7 @@
     ends = [0]
     for a in arrays:
         ends.append(ends[-1] + a.size)
-    subtotal = lax.psum(jnp.concatenate([a.ravel() for a in arrays]), axis)
+    subtotal = jnp.sum(lax.all_gather(jnp.concatenate([a.ravel() for a in arrays]), axis), axis=0)
     return tuple((subtotal[b:e].reshape(a.shape) for a, b, e in zip(arrays, ends, ends[1:])))
 
 

time: 392 us -> 302 us (0.77)
  waiting for transfers between devices: 228 us -> 148 us
  blocking collectives: 51.9 us -> 13.5 us
  starting transfers between devices: 23.6 us -> 34.4 us
  other arithmetic: 4.95 us -> 15.3 us
  local copies, waits for them, and re-layouts: 5.3 us -> 12.2 us
    psum x1 -> x0, waiting for transfers between devices: 70.1 us -> none  [together(): subtotal = lax.psum(jnp.concatenate([a.ravel() for a in arrays]), axis)]
    all_to_all x1, waiting for transfers between devices: 95.4 us -> 48.2 us  [shards(): lax.all_to_all(stacked.astype(jnp.bfloat16), SP, split_axis=0, concat_axi...]
    all_to_all x1 -> x0, blocking collectives: 38.4 us -> none  [sum_at_owner(): lax.all_to_all(pieces, axis, split_axis=0, concat_axis=0, tiled=True)]
    all_gather x0 -> x1, waiting for transfers between devices: none -> 23.5 us  [together(): lax.all_gather(jnp.concatenate([a.ravel() for a in arrays]), axis)]
    all_to_all x0 -> x1, waiting for transfers between devices: none -> 14 us  [sum_at_owner(): lax.all_to_all(pieces, axis, split_axis=0, concat_axis=0, tiled=True)]
    reduce_sum x0 -> x1, other arithmetic: none -> 10.3 us  [together(): jnp.sum(lax.all_gather(jnp.concatenate([a.ravel() for a in arrays]), axis...]
    all_gather x0 -> x1, local copies, waits for them, and re-layouts: none -> 5.92 us  [together(): lax.all_gather(jnp.concatenate([a.ravel() for a in arrays]), axis)]
    all_to_all x0 -> x1, starting transfers between devices: none -> 5.84 us  [sum_at_owner(): lax.all_to_all(pieces, axis, split_axis=0, concat_axis=0, tiled=True)]
  transfers between devices with their start and end apart: 4 -> 5, of which waited for: 4 -> 5; matrix products, arithmetic and copies ran while one was open for 2% -> 9% of each run, Pallas kernels for 0% -> 0%
where the time goes in v1:
time: 302 us; the launch traced here: 300 us
  waiting for transfers between devices  148 us (49%)
  matrix products  62.7 us (21%)
  starting transfers between devices  34.4 us (11%)
  other arithmetic  15.3 us (5%)
  between operations  14.2 us (5%)
  blocking collectives  13.5 us (4%)
  local copies, waits for them, and re-layouts  12.2 us (4%)
    all_to_all x1, waiting for transfers between devices, shards(): lax.all_to_all(stacked.astype(jnp.bfloat16), SP, split_axis=0, concat_axi...  48.2 us
    all_gather x1, waiting for transfers between devices, gather_axes(): value = lax.all_gather(value, axis, axis=dim, tiled=True)  47.4 us
    dot_general x18, matrix products, contract_cols(): lax.dot_general(left, right, (((1,), (1,)), ((), ())), preferred_element_...  27.9 us
    dot_general x17, matrix products, contract_rows(): lax.dot_general(left, right, (((0,), (0,)), ((), ())), preferred_element_...  25.7 us
    all_gather x1, waiting for transfers between devices, together(): lax.all_gather(jnp.concatenate([a.ravel() for a in arrays]), axis)  23.5 us
    all_to_all x1, starting transfers between devices, copy_for_each(): lax.all_to_all(jnp.broadcast_to(value[None], (size, *value.shape)), axis,...  18.2 us
    all_to_all x1, waiting for transfers between devices, copy_for_each(): lax.all_to_all(jnp.broadcast_to(value[None], (size, *value.shape)), axis,...  14.7 us
    all_to_all x1, waiting for transfers between devices, sum_at_owner(): lax.all_to_all(pieces, axis, split_axis=0, concat_axis=0, tiled=True)  14 us
  transfers between devices with their start and end apart: 5, of which 5 were waited for; matrix products, arithmetic and copies ran while one was open for 9% of the time, Pallas kernels for 0%

profile of v1, /device:TPU:6, one launch (start us, length us, event | category | flops | bytes accessed | tf_op | source)
XLA Modules:
  0.0 300.4 jit_solution(15039779766509774132)
XLA Ops:
  7.2 0.8 pad_maximum_fusion.1
  8.1 13.5 %all_gather.12 = bf16[2,512,128]{2,1,0:T(8,128)(2,1)} all-gather(bf16[2,128,128]{2,1,0:T(8,128)(2,1)S(1)} %pad_maximum_fusion.1), channel_id=1, replica_groups=mesh['sp_0'=16,'sp_1'=4,'tp'=8] {'sp_1'}, dimensions={1}, use_global_device_ids=true | all-gather | bytes 327680 | tf_op jit(solution)/shard_map/all_gather | solution.py:34
  21.6 0.9 multiply_reduce_fusion
  23.8 18.2 %all-to-all-start = ((f32[64,2,128,1]{2,1,3,0:T(2,128)}), f32[64,2,128,1]{2,1,3,0:T(2,128)S(1)}, u32[]{:S(2)}, u32[]{:S(2)}) async-start(f32[64,2,128,1]{2,1,3,0:T(2,128)} %broadcast_in_dim.13), calls=%async_computation | async-start | bytes 131072 | tf_op jit(solution)/shard_map/all_to_all | solution.py:16
  42.1 1.0 constant_dynamic-slice_fusion.2
  43.0 14.7 %all-to-all-done = f32[64,2,128,1]{2,1,3,0:T(2,128)S(1)} async-done(((f32[64,2,128,1]{2,1,3,0:T(2,128)}), f32[64,2,128,1]{2,1,3,0:T(2,128)S(1)}, u32[]{:S(2)}, u32[]{:S(2)}) %all-to-all-start) | async-done | bytes 65568 | tf_op jit(solution)/shard_map/all_to_all | solution.py:16
  57.8 47.4 %all-gather.4.cloned.1.call-done = bf16[2,8192,128]{2,1,0:T(8,128)(2,1)} async-done(((bf16[2,512,128]{2,1,0:T(8,128)(2,1)}), bf16[2,8192,128]{2,1,0:T(8,128)(2,1)}) %all-gather.4.cloned.1.call-update) | async-done | bytes 4194320 | tf_op jit(solution)/shard_map/all_gather | solution.py:34
  105.3 1.5 broadcast_in_dim.11
  106.8 59.0 %while.19 = (s32[]{:T(128)}, bf16[8192,128]{1,0:T(8,128)(2,1)}, f32[512,256]{1,0:T(8,128)S(1)}, f32[512,256]{1,0:T(8,128)S(1)}, bf16[2,8192,128]{2,1,0:T(8,128)(...) while((s32[]{:T(128)}, bf16[8192,128]{1,0:T(8,128)(2,1)}, ...), condition=%wide.region_2.3_spmd, body=%wide.region_1.2_spmd.sunk | while | flops 675938304 | bytes 12481763 | solution.py:139
  106.8 1.4 fusion.41
  108.2 1.7 fusion.43
  109.9 1.6 multiply_convert_fusion.2
  111.5 1.4 fusion.42
  113.0 1.2 convolution_dynamic-update-slice_fusion.2
  114.2 1.4 fusion.41
  115.5 1.7 fusion.43
  117.3 1.7 multiply_convert_fusion.2
  118.9 1.4 fusion.42
  120.4 1.1 convolution_dynamic-update-slice_fusion.2
  121.5 1.4 fusion.41
  122.9 1.7 fusion.43
  124.6 1.7 multiply_convert_fusion.2
  126.3 1.4 fusion.42
  127.7 1.2 convolution_dynamic-update-slice_fusion.2
  128.9 1.4 fusion.41
  130.3 1.7 fusion.43
  132.0 1.7 multiply_convert_fusion.2
  133.7 1.4 fusion.42
  135.1 1.2 convolution_dynamic-update-slice_fusion.2
  136.3 1.4 fusion.41
  137.7 1.7 fusion.43
  139.4 1.7 multiply_convert_fusion.2
  141.1 1.4 fusion.42
  142.5 1.1 convolution_dynamic-update-slice_fusion.2
  143.6 1.4 fusion.41
  145.0 1.7 fusion.43
  146.8 1.7 multiply_convert_fusion.2
  148.4 1.4 fusion.42
  149.9 1.1 convolution_dynamic-update-slice_fusion.2
  151.0 1.4 fusion.41
  152.4 1.7 fusion.43
  154.1 1.7 multiply_convert_fusion.2
  155.8 1.4 fusion.42
  157.2 1.1 convolution_dynamic-update-slice_fusion.2
  158.4 1.4 fusion.41
  159.7 1.7 fusion.43
  161.5 1.7 multiply_convert_fusion.2
  163.1 1.4 fusion.42
  164.6 1.1 convolution_dynamic-update-slice_fusion.2
  166.2 0.8 pad_maximum_fusion
  167.1 10.3 %all-to-all-start.1 = ((bf16[64,128,128]{2,1,0:T(8,128)(2,1)}), bf16[64,128,128]{2,1,0:T(8,128)(2,1)S(1)}, u32[]{:S(2)}, u32[]{:S(2)}) async-start(bf16[64,128,128]{2,1,0:T(8,128)(2,1)} %bitcast.58), calls=%async_computation.1 | async-start | bytes 4194304 | tf_op jit(solution)/shard_map/all_to_all | solution.py:141
  177.4 23.5 %all-gather.6.cloned.1.call-done = bf16[2097152]{0:T(1024)(128)(2,1)} async-done(((bf16[262144]{0:T(1024)(128)(2,1)}), bf16[2097152]{0:T(1024)(128)(2,1)}) %all-gather.6.cloned.1.call-update) | async-done | bytes 4194320 | tf_op jit(solution)/shard_map/all_gather | solution.py:42
  200.9 5.9 %reshape.50 = bf16[8,262144]{1,0:T(8,128)(2,1)} reshape(bf16[2097152]{0:T(1024)(128)(2,1)} %all-gather.6.cloned.1.call-done) | data formatting | bytes 8388608 | tf_op jit(solution)/shard_map/all_gather | solution.py:42
  206.8 10.3 %reduce_sum.41 = bf16[262144]{0:T(1024)(128)(2,1)S(1)} reduce(bf16[8,262144]{1,0:T(8,128)(2,1)} %reshape.50, bf16[]{:T(256)} %constant.86.clone.1), dimensions={0}, to_apply=%region_4.5 | reduce | flops 1835008 | bytes 4718594 | tf_op jit(solution)/shard_map/reduce_sum | solution.py:42
  217.1 0.7 fusion.13
  217.9 1.0 slice.63
  219.3 0.8 reshape.49
  220.0 48.2 %all-to-all-done.1 = bf16[64,128,128]{2,1,0:T(8,128)(2,1)S(1)} async-done(((bf16[64,128,128]{2,1,0:T(8,128)(2,1)}), bf16[64,128,128]{2,1,0:T(8,128)(2,1)S(1)}, u32[]{:S(2)}, u32[]{:S(2)}) %all-to-all-start.1) | async-done | bytes 2097184 | tf_op jit(solution)/shard_map/all_to_all | solution.py:141
  268.3 5.8 %all-to-all-start.2 = ((bf16[64,4,512]{2,1,0:T(4,128)(2,1)}), bf16[64,4,512]{2,1,0:T(4,128)(2,1)S(1)}, u32[]{:S(2)}, u32[]{:S(2)}) async-start(bf16[64,4,512]{2,1,0:T(4,128)(2,1)} %reshape.49), calls=%async_computation.2 | async-start | bytes 524288 | tf_op jit(solution)/shard_map/all_to_all | solution.py:53
  274.2 1.4 fusion.14
  275.6 2.3 convolution_add_fusion.2
  277.8 0.9 convert_reduce_fusion
  278.8 14.0 %all-to-all-done.2 = bf16[64,4,512]{2,1,0:T(4,128)(2,1)S(1)} async-done(((bf16[64,4,512]{2,1,0:T(4,128)(2,1)}), bf16[64,4,512]{2,1,0:T(4,128)(2,1)S(1)}, u32[]{:S(2)}, u32[]{:S(2)}) %all-to-all-start.2) | async-done | bytes 262176 | tf_op jit(solution)/shard_map/all_to_all | solution.py:53
  292.8 0.7 convert_reduce_fusion.1
  (27 shorter events, 2.4 us)
Async XLA Ops:
  7.2 211.8 %copy-start = (bf16[512,512]{1,0:T(8,128)(2,1)S(1)}, bf16[512,512]{1,0:T(8,128)(2,1)}, u32[]{:S(2)}) copy-start(bf16[512,512]{1,0:T(8,128)(2,1)} %param.15) | copy-start | bytes 1572868
  7.2 98.0 %all-gather.4.cloned.1.call-start = ((), (), s32[]{:S(2)}) async-start(), calls=%async_computation.3 | async-start | bytes 4456448 | tf_op jit(solution)/shard_map/all_gather | solution.py:34
  23.8 34.0 %all-to-all-start = ((f32[64,2,128,1]{2,1,3,0:T(2,128)}), f32[64,2,128,1]{2,1,3,0:T(2,128)S(1)}, u32[]{:S(2)}, u32[]{:S(2)}) async-start(f32[64,2,128,1]{2,1,3,0:T(2,128)} %broadcast_in_dim.13), calls=%async_computation | async-start | bytes 131072 | tf_op jit(solution)/shard_map/all_to_all | solution.py:16
  42.0 158.9 %all-gather.6.cloned.1.call-start = ((), (), s32[]{:S(2)}) async-start(), calls=%async_computation.4 | async-start | bytes 4718592 | tf_op jit(solution)/shard_map/all_gather | solution.py:42
  167.1 101.2 %all-to-all-start.1 = ((bf16[64,128,128]{2,1,0:T(8,128)(2,1)}), bf16[64,128,128]{2,1,0:T(8,128)(2,1)S(1)}, u32[]{:S(2)}, u32[]{:S(2)}) async-start(bf16[64,128,128]{2,1,0:T(8,128)(2,1)} %bitcast.58), calls=%async_computation.1 | async-start | bytes 4194304 | tf_op jit(solution)/shard_map/all_to_all | solution.py:141
  218.9 55.2 %copy-start.1 = (bf16[512,256]{1,0:T(8,128)(2,1)}, bf16[512,256]{1,0:T(8,128)(2,1)S(1)}, u32[]{:S(2)}) copy-start(bf16[512,256]{1,0:T(8,128)(2,1)S(1)} %slice.63) | copy-start | bytes 786436
  268.3 24.5 %all-to-all-start.2 = ((bf16[64,4,512]{2,1,0:T(4,128)(2,1)}), bf16[64,4,512]{2,1,0:T(4,128)(2,1)S(1)}, u32[]{:S(2)}, u32[]{:S(2)}) async-start(bf16[64,4,512]{2,1,0:T(4,128)(2,1)} %reshape.49), calls=%async_computation.2 | async-start | bytes 524288 | tf_op jit(solution)/shard_map/all_to_all | solution.py:53
Sparse Core Ops, SparseCore 0:
  21.7 83.4 all-gather.3
  167.2 33.6 all-gather.5
